TPU v7x, 32 devices: a whole 2x2x4 slice. The times are simulated.
32 devices in a mesh: sp: 8 (over z, y), tp: 4 (over x, core).
Axes of the slice: x: 2, y: 2, z: 4, core: 2. Of those that a mesh axis runs over, the one named last changes fastest.
Arguments:
- layer_input: bfloat16 [6144, 2048], P('sp', 'tp'), may hold values from -6 to 6
- input_norm_gain: bfloat16 [2048], replicated, may hold values from 0.099609375 to 1.8984375
- query_weight: bfloat16 [2048, 2048], P(None, 'tp'), may hold values from -0.125 to 0.125
- forget_weight: bfloat16 [2048, 2048], P(None, 'tp'), may hold values from -0.125 to 0.125
- value_matrix: bfloat16 [2048, 2048], P(None, 'tp'), may hold values from -0.125 to 0.125
- output_gate_weight: bfloat16 [2048, 2048], P(None, 'tp'), may hold values from -0.125 to 0.125
- after_gate_weight: bfloat16 [2048, 2048], P(None, 'tp'), may hold values from -0.125 to 0.125
- before_gate_weight: bfloat16 [2048, 2048], P(None, 'tp'), may hold values from -0.125 to 0.125
- convolution_input_weight: bfloat16 [2048, 2048], P(None, 'tp'), may hold values from -0.125 to 0.125
- forget_minimum: float32 [2048], P('tp'), may hold values from 0.95 to 0.9999837
- surge_log_decay: float32 [6144, 2048], P('sp', 'tp'), may hold values from -2.2 to 0
- convolution_kernel: bfloat16 [3, 2048], P(None, 'tp'), may hold values from -4 to 4
- head_norm_gain: bfloat16 [128], replicated, may hold values from 0.099609375 to 1.8984375
- starting_state: float32 [16, 128, 128], P('tp', 'sp'), may hold values from -0.09375 to 0.09375
- recurrence_output_weight: bfloat16 [2048, 2048], P('tp'), may hold values from -0.09375 to 0.09375
- convolution_output_weight: bfloat16 [2048, 2048], P('tp'), may hold values from -0.09375 to 0.09375
- output_norm_gain: bfloat16 [2048], replicated, may hold values from 0.099609375 to 1.8984375
Outputs:
- layer_out: bfloat16 [6144, 2048], P(('sp', 'tp'))
All inputs are finite; a program needn't handle non-finite values.
Results may differ from a plain program's by a relative error of at most 0.014.
Values may be sent and summed in bfloat16 or wider, within the bound.
A program may use at most 128 MiB of HBM per device.

v0:
```python
import functools

import jax
import jax.numpy as jnp
from jax import lax
from jax.experimental import pallas as pl
from jax.experimental.pallas import tpu as pltpu
from jax.sharding import PartitionSpec as P

DK = 128
DV = 128
CK = 3
BLK = 64
LANES = 128
PAD = 8


EPS = 1e-06
F32 = jnp.float32
BF16 = jnp.bfloat16
MESH = pl.DeviceIdType.MESH


def rms_scale(value_rows):
    return lax.rsqrt(jnp.mean(value_rows * value_rows, axis=-1, keepdims=True) + EPS)


def nt_dot(a, b):
    return lax.dot_general(a, b, (((1,), (1,)), ((), ())), preferred_element_type=F32)


def tn_dot(a, b):
    return lax.dot_general(a, b, (((0,), (0,)), ((), ())), preferred_element_type=F32)


def tp_places():
    me = lax.axis_index("tp")
    pair, core = me // 2, me % 2
    partner = 2 * pair + (1 - core)
    cross = 2 * (1 - pair) + core
    far = 2 * (1 - pair) + (1 - core)
    return me, partner, cross, far


def aligned(start, size):
    return pl.ds(pl.multiple_of(start, size), size)


def aligned_by(start, step, size):
    return pl.ds(pl.multiple_of(start, step), size)


def row_of(ref):
    lines = ref[...].astype(F32)
    return jnp.concatenate([lines[i : i + 1, :] for i in range(lines.shape[0])], axis=1)


def layer_kernel(
    heads,
    chunk,
    pieces,
    x_hbm,
    gain_hbm,
    wq_hbm,
    wf_hbm,
    wv_hbm,
    wpre_hbm,
    wconv_hbm,
    wpost_hbm,
    wout_hbm,
    surge_hbm,
    fmin_hbm,
    taps_hbm,
    hgain_hbm,
    start_hbm,
    wr_hbm,
    wc_hbm,
    ogain_hbm,
    out_ref,
    wbuf,
    xg,
    nb,
    surge,
    part,
    shift,
    st,
    run,
    pack,
    decs,
    land,
    land_decay,
    ent,
    back,
    gate,
    post,
    mix,
    halo,
    wr,
    wc,
    acc,
    pbuf,
    prcv,
    cbuf,
    crcv,
    land_state,
    gain_ref,
    fmin_ref,
    taps_ref,
    hgain_ref,
    start_ref,
    ogain_ref,
    lsem,
    csend,
    crecv,
    psend,
    precv,
    fsend,
    frecv,
    s1,
    r1,
    sd,
    rd,
    s2,
    r2,
    hs,
    hr,
    ps,
    pr,
    cs,
    cr,
    ready,
):
    peers, tokens, width = xg.shape
    steps = tokens // chunk
    sp = lax.axis_size("sp")
    seq = lax.axis_index("sp")
    quarter = tokens // peers
    size = quarter // pieces
    me, partner, cross, far = tp_places()
    sources = (wq_hbm, wf_hbm, wv_hbm, wpre_hbm, wconv_hbm, wpost_hbm, wout_hbm)

    x_copy = pltpu.make_async_copy(x_hbm, xg.at[me], lsem.at[0])
    surge_copy = pltpu.make_async_copy(surge_hbm, surge, lsem.at[1])
    wr_copy = pltpu.make_async_copy(wr_hbm, wr, lsem.at[2])
    wc_copy = pltpu.make_async_copy(wc_hbm, wc, lsem.at[3])

    def weight_copy(j):
        return pltpu.make_async_copy(sources[j], wbuf.at[j], lsem.at[4 + j])

    x_copy.start()
    smalls = (
        (gain_hbm, gain_ref),
        (fmin_hbm, fmin_ref),
        (taps_hbm, taps_ref),
        (hgain_hbm, hgain_ref),
        (start_hbm, start_ref),
        (ogain_hbm, ogain_ref),
    )
    small_copies = [
        pltpu.make_async_copy(src, dst, lsem.at[11 + i]) for i, (src, dst) in enumerate(smalls)
    ]
    barrier = pltpu.get_barrier_semaphore()
    for other in (partner, cross):
        pl.semaphore_signal(barrier, inc=1, device_id={"tp": other}, device_id_type=MESH)
    for off in range(1, sp):
        to = (seq + off) % sp

        @pl.when(to > seq)
        def _():
            pl.semaphore_signal(barrier, inc=1, device_id={"sp": to}, device_id_type=MESH)

    for copy in small_copies:
        copy.start()
    for j in range(3):
        weight_copy(j).start()
    surge_copy.start()
    with jax.named_scope("entry"):
        x_copy.wait()
        pl.semaphore_wait(barrier, 2 + seq)

    def give(src, dst, send, recv, to):
        return pltpu.make_async_remote_copy(
            src_ref=src,
            dst_ref=dst,
            send_sem=send,
            recv_sem=recv,
            device_id=to,
            device_id_type=MESH,
        )

    def hop(step, slot, to, send, recv):
        rows = aligned(step * chunk, chunk)
        return give(xg.at[slot, rows], xg.at[slot, rows], send.at[step], recv.at[step], {"tp": to})

    for step in range(steps):
        hop(step, me, cross, csend, crecv).start()
    for step in range(steps):
        hop(step, me, partner, psend, precv).start()
    for j in range(3, 7):
        weight_copy(j).start()
    wc_copy.start()
    wr_copy.start()

    def state_hop(src, dst, slot, to, send, recv):
        return give(src.at[to], dst.at[slot], send.at[to], recv.at[slot], {"sp": to})

    def decay_hop(slot, to):
        return give(decs, land_decay.at[slot], sd.at[to], rd.at[slot], {"sp": to})

    for off in range(1, sp):
        to = (seq + off) % sp

        @pl.when(to < seq)
        def _():
            pl.semaphore_signal(ready, inc=1, device_id={"sp": to}, device_id_type=MESH)

    for copy in small_copies:
        copy.wait()
    running = [start_ref[h] for h in range(heads)]
    for h in range(heads):
        ent[0, h] = running[h].astype(BF16)

    @pl.when(seq > 0)
    def _():
        state_hop(ent, back, seq, 0, s2, r2).start()

    st[...] = jnp.zeros_like(st)
    run[...] = jnp.zeros_like(run)
    gain = row_of(gain_ref)
    row = lax.broadcasted_iota(jnp.int32, (BLK, BLK), 0)
    col = lax.broadcasted_iota(jnp.int32, (BLK, BLK), 1)
    causal = col <= row
    middle = (causal.astype(F32) - (col < BLK // 2).astype(F32)).astype(BF16)
    middle = jnp.concatenate([middle] * 3, axis=1)

    def block(rows, query_raw, forget_raw, values):
        forget = forget_raw.astype(F32)
        keys = (1.0 - fmin_ref[...]) * jax.nn.sigmoid(-forget)
        logs = jnp.log1p(-keys) + surge[rows, :]
        high = logs.astype(BF16)
        rest = logs - high.astype(F32)
        next_term = rest.astype(BF16)
        low = (rest - next_term.astype(F32)).astype(BF16)
        terms = jnp.concatenate([high, next_term, low], axis=0)
        rel = jnp.dot(middle, terms, preferred_element_type=F32)
        mid = logs[0:1, :] - rel[0:1, :]
        tail = rel[BLK - 1 : BLK, :]
        raw = query_raw.astype(F32)
        queries = raw * jax.nn.sigmoid(raw) * DK ** (-0.5)
        q_mid = queries * jnp.exp(rel)
        k_mid = keys * jnp.exp(-rel)
        q_in = q_mid * jnp.exp(mid)
        k_out = (k_mid * jnp.exp(tail)).astype(BF16)
        whole = jnp.exp(mid + tail)
        shift[rows, :] = (q_in * jnp.exp(run[...])).astype(BF16)
        run[...] = run[...] + mid + tail
        q_mid = q_mid.astype(BF16)
        k_mid = k_mid.astype(BF16)
        q_in = q_in.astype(BF16)
        for h in range(heads):
            ch = slice(h * DK, (h + 1) * DK)
            scores = jnp.where(causal, nt_dot(q_mid[:, ch], k_mid[:, ch]), 0.0).astype(BF16)
            before = st[h]
            part[rows, ch] = jnp.dot(
                scores, values[:, ch], preferred_element_type=F32
            ) + nt_dot(q_in[:, ch], before.astype(BF16))
            st[h] = before * whole[:, ch] + tn_dot(values[:, ch], k_out[:, ch])

    def project(rows, j):
        return jnp.dot(nb[rows, :], wbuf[j], preferred_element_type=F32).astype(BF16)

    lag = me % 2

    @pl.loop(0, steps + lag)
    def _(step):
        @pl.when(step < steps)
        def _():
            with jax.named_scope("wait_cross"):
                hop(step, cross, cross, csend, crecv).wait_recv()
            hop(step, cross, partner, fsend, frecv).start()

        @pl.when(step >= lag)
        def _():
            now = step - lag
            with jax.named_scope("wait_forward"):
                hop(now, partner, partner, psend, precv).wait_recv()
                hop(now, far, partner, fsend, frecv).wait_recv()
            rows = aligned(now * chunk, chunk)
            total = jnp.zeros((chunk, 1), F32)
            for s in range(peers):
                piece = xg[s, rows].astype(F32)
                total = total + jnp.sum(piece * piece, axis=-1, keepdims=True)
            scale = lax.rsqrt(total / (peers * width) + EPS)
            for s in range(peers):
                cols = slice(s * width, (s + 1) * width)
                nb[rows, cols] = (xg[s, rows].astype(F32) * scale * gain[:, cols]).astype(BF16)

            @pl.when(now == 0)
            def _():
                surge_copy.wait()
                for j in range(3):
                    weight_copy(j).wait()

            query_raw, forget_raw, value_raw = (project(rows, j) for j in range(3))
            for b in range(chunk // BLK):
                inner = slice(b * BLK, (b + 1) * BLK)
                block(
                    aligned(now * chunk + b * BLK, BLK),
                    query_raw[inner],
                    forget_raw[inner],
                    value_raw[inner],
                )

    piece = DK // sp
    packing = jax.named_scope("pack")
    packing.__enter__()
    whole = jnp.exp(run[...])
    for h in range(heads):
        ch = slice(h * DK, (h + 1) * DK)
        decs[h : h + 1, :] = whole[:, ch]
        state = st[h].T
        for p in range(sp):
            pack[p, h] = state[p * piece : (p + 1) * piece].astype(BF16)

    @pl.when(seq < sp - 1)
    def _():
        pl.semaphore_wait(ready, sp - 1 - seq)
        for off in range(1, sp):
            to = (seq + off) % sp
            decay_hop(seq, to).start()
            state_hop(pack, land, seq, to, s1, r1).start()

    land[seq] = pack[seq]
    land_decay[seq] = decs[...]
    packing.__exit__(None, None, None)
    gates = jax.named_scope("gates_a")
    gates.__enter__()
    for j in range(3, 7):
        weight_copy(j).wait()

    def halo_hop():
        return give(
            mix.at[pl.ds(tokens, PAD)], halo, hs.at[0], hr.at[0], {"sp": (seq + 1) % sp}
        )

    wide = 2 * chunk if tokens % (2 * chunk) == 0 else chunk

    @pl.loop(0, tokens // wide)
    def _(i):
        rows = aligned(i * wide, wide)
        mix[pl.ds(pl.multiple_of(PAD + i * wide, PAD), wide), :] = project(rows, 3).astype(
            F32
        ) * project(rows, 4).astype(F32)

    @pl.when(seq < sp - 1)
    def _():
        halo_hop().start()

    def prepare(which):
        rows = aligned(which * quarter, quarter)
        post[rows, :] = project(rows, 5)
        gate[rows, :] = project(rows, 6)

    def convolve(which):
        rows = aligned(which * quarter, quarter)
        near = mix[aligned_by(which * quarter, PAD, quarter + PAD), :]
        total = None
        for j in range(CK):
            first = PAD + j - (CK - 1)
            term = near[first : first + quarter, :] * taps_ref[j : j + 1, :].astype(F32)
            total = term if total is None else total + term
        conv = (post[rows, :].astype(F32) * total).astype(BF16)
        acc[rows, :] = jnp.dot(conv, wc[...], preferred_element_type=F32)

    prepare(far)
    gates.__exit__(None, None, None)
    with jax.named_scope("wait_states"):
        for off in range(1, sp):
            src = (seq + sp - off) % sp

            @pl.when(src < sp - 1)
            def _():
                decay_hop(src, (seq + off) % sp).wait_recv()
                state_hop(pack, land, src, (seq + off) % sp, s1, r1).wait_recv()

    gates = jax.named_scope("gates_b")
    gates.__enter__()
    lane = lax.broadcasted_iota(jnp.int32, (piece, DK), 1)
    pick = lane == seq * piece + lax.broadcasted_iota(jnp.int32, (piece, DK), 0)
    for i in range(sp - 1):
        for h in range(heads):
            line = jnp.broadcast_to(land_decay[i, h : h + 1, :], (piece, DK))
            decay = jnp.sum(jnp.where(pick, line, 0.0), axis=-1, keepdims=True)
            running[h] = decay * running[h] + land[i, h].astype(F32)
            ent[i + 1, h] = running[h].astype(BF16)
    back[seq] = ent[seq]
    for off in range(1, sp):
        to = (seq + off) % sp

        @pl.when(to > 0)
        def _():
            state_hop(ent, back, seq, to, s2, r2).start()

    prepare(cross)
    mix[0:PAD, :] = jnp.zeros((PAD, width), F32)

    @pl.when(seq > 0)
    def _():
        halo_hop().wait_recv()
        mix[0:PAD, :] = halo[...]

    wc_copy.wait()
    wr_copy.wait()
    convolve(far)
    convolve(cross)
    gates.__exit__(None, None, None)
    with jax.named_scope("wait_entering"):
        for off in range(1, sp):
            src = (seq + sp - off) % sp
            state_hop(ent, back, src, (seq + off) % sp, s2, r2).wait_recv()
    for h in range(heads):
        land_state[h] = jnp.concatenate(
            [back[i, h].astype(F32) for i in range(sp)], axis=0
        ).astype(BF16)

    def mixed(which, s):
        rows = aligned(which * quarter + s * size, size)
        gated = []
        for h in range(heads):
            ch = slice(h * DV, (h + 1) * DV)
            recur = part[rows, ch] + jnp.dot(
                shift[rows, ch], land_state[h], preferred_element_type=F32
            )
            g = gate[rows, ch].astype(F32)
            gated.append(
                (
                    recur * rms_scale(recur) * hgain_ref[...].astype(F32) * (g * jax.nn.sigmoid(g))
                ).astype(BF16)
            )
        rec = jnp.concatenate(gated, axis=1)
        return acc[rows, :] + jnp.dot(rec, wr[...], preferred_element_type=F32)

    def put(which, s):
        rows = aligned(which * quarter + s * size, size)
        acc[rows, :] = mixed(which, s)

    def partner_hop(i):
        return give(pbuf.at[i], prcv.at[i], ps.at[i], pr.at[i], {"tp": partner})

    def cross_hop(i):
        return give(cbuf.at[i], crcv.at[i], cs.at[i], cr.at[i], {"tp": cross})

    def share(which, s, slot):
        pbuf[slot] = mixed(which, s).astype(BF16)
        partner_hop(slot).start()

    def forward(s):
        partner_hop(s).wait_recv()
        rows = aligned(cross * quarter + s * size, size)
        cbuf[s] = (acc[rows, :] + prcv[s].astype(F32)).astype(BF16)
        cross_hop(s).start()

    sums = jax.named_scope("sums")
    sums.__enter__()

    @pl.loop(0, pieces + 1)
    def _(s):
        @pl.when(s < pieces)
        def _():
            share(far, s, s)

        @pl.when(s > 0)
        def _():
            forward(s - 1)

        @pl.when(s < pieces)
        def _():
            put(cross, s)

    prepare(partner)
    convolve(partner)
    prepare(me)
    convolve(me)

    @pl.loop(0, pieces)
    def _(s):
        share(partner, s, pieces + s)
        put(me, s)

    sums.__exit__(None, None, None)
    last = jax.named_scope("last")
    last.__enter__()
    ogain = row_of(ogain_ref)

    @pl.loop(0, pieces)
    def _(s):
        partner_hop(pieces + s).wait_recv()
        cross_hop(s).wait_recv()
        rows = aligned(me * quarter + s * size, size)
        total = acc[rows, :] + prcv[pieces + s].astype(F32) + crcv[s].astype(F32)
        out_ref[aligned(s * size, size), :] = (total * rms_scale(total) * ogain).astype(BF16)

    last.__exit__(None, None, None)
    for step in range(steps):
        hop(step, me, cross, csend, crecv).wait_send()
        hop(step, me, partner, psend, precv).wait_send()
        hop(step, cross, partner, fsend, frecv).wait_send()
    for off in range(1, sp):
        to = (seq + off) % sp

        @pl.when(seq < sp - 1)
        def _():
            decay_hop(seq, to).wait_send()
            state_hop(pack, land, seq, to, s1, r1).wait_send()

        state_hop(ent, back, seq, to, s2, r2).wait_send()

    @pl.when(seq < sp - 1)
    def _():
        halo_hop().wait_send()

    for i in range(2 * pieces):
        partner_hop(i).wait_send()
    for i in range(pieces):
        cross_hop(i).wait_send()


def shards(
    layer_input,
    input_norm_gain,
    query_weight,
    forget_weight,
    value_matrix,
    output_gate_weight,
    after_gate_weight,
    before_gate_weight,
    convolution_input_weight,
    forget_minimum,
    surge_log_decay,
    convolution_kernel,
    head_norm_gain,
    starting_state,
    recurrence_output_weight,
    convolution_output_weight,
    output_norm_gain,
):
    sp, tp = lax.axis_size("sp"), lax.axis_size("tp")
    tokens, width = layer_input.shape
    wide = recurrence_output_weight.shape[1]
    depth, cols = query_weight.shape
    heads = cols // DV
    chunk = 128 if tokens % 128 == 0 else BLK
    steps = tokens // chunk
    quarter = tokens // tp
    pieces = 4 if quarter % 64 == 0 else 2
    size = quarter // pieces
    shares = (sp, heads, DK // sp, DV)
    vmem = pl.BlockSpec(memory_space=pltpu.VMEM)
    hbm = pl.BlockSpec(memory_space=pltpu.HBM)
    dma = pltpu.SemaphoreType.DMA
    return pl.pallas_call(
        functools.partial(layer_kernel, heads, chunk, pieces),
        out_shape=pltpu.VMEM((quarter, wide), BF16),
        in_specs=[hbm] * 17,
        out_specs=vmem,
        scratch_shapes=[
            pltpu.VMEM((7, depth, cols), BF16),
            pltpu.VMEM((tp, tokens, width), BF16),
            pltpu.VMEM((tokens, depth), BF16),
            pltpu.VMEM((tokens, cols), F32),
            pltpu.VMEM((tokens, cols), F32),
            pltpu.VMEM((tokens, cols), BF16),
            pltpu.VMEM((heads, DV, DK), F32),
            pltpu.VMEM((1, cols), F32),
            pltpu.VMEM(shares, BF16),
            pltpu.VMEM((heads, DK), F32),
            pltpu.VMEM(shares, BF16),
            pltpu.VMEM((sp, heads, DK), F32),
            pltpu.VMEM(shares, BF16),
            pltpu.VMEM(shares, BF16),
            pltpu.VMEM((tokens, cols), BF16),
            pltpu.VMEM((tokens, cols), BF16),
            pltpu.VMEM((tokens + PAD, cols), F32),
            pltpu.VMEM((PAD, cols), F32),
            pltpu.VMEM((cols, wide), BF16),
            pltpu.VMEM((cols, wide), BF16),
            pltpu.VMEM((tokens, wide), F32),
            pltpu.VMEM((2 * pieces, size, wide), BF16),
            pltpu.VMEM((2 * pieces, size, wide), BF16),
            pltpu.VMEM((pieces, size, wide), BF16),
            pltpu.VMEM((pieces, size, wide), BF16),
            pltpu.VMEM((heads, DK, DV), BF16),
            pltpu.VMEM((depth // LANES, LANES), BF16),
            pltpu.VMEM((1, cols), F32),
            pltpu.VMEM((CK, cols), BF16),
            pltpu.VMEM((1, DV), BF16),
            pltpu.VMEM(starting_state.shape, F32),
            pltpu.VMEM((wide // LANES, LANES), BF16),
            dma((17,)),
        ]
        + [dma((steps,))] * 6
        + [dma((sp,))] * 6
        + [dma((1,))] * 2
        + [dma((2 * pieces,))] * 2
        + [dma((pieces,))] * 2
        + [pltpu.SemaphoreType.REGULAR],
        compiler_params=pltpu.CompilerParams(collective_id=0, has_side_effects=True, vmem_limit_bytes=56 * 1024 * 1024),
        name="layer",
    )(
        layer_input,
        input_norm_gain.reshape(-1, LANES),
        query_weight,
        forget_weight,
        value_matrix,
        before_gate_weight,
        convolution_input_weight,
        after_gate_weight,
        output_gate_weight,
        surge_log_decay,
        forget_minimum[None, :],
        convolution_kernel,
        head_norm_gain[None, :],
        starting_state,
        recurrence_output_weight,
        convolution_output_weight,
        output_norm_gain.reshape(-1, LANES),
    )


def solution(mesh):
    return jax.shard_map(
        shards,
        mesh=mesh,
        in_specs=(
            P("sp", "tp"),
            P(),
            P(None, "tp"),
            P(None, "tp"),
            P(None, "tp"),
            P(None, "tp"),
            P(None, "tp"),
            P(None, "tp"),
            P(None, "tp"),
            P("tp"),
            P("sp", "tp"),
            P(None, "tp"),
            P(),
            P("tp", "sp", None),
            P("tp", None),
            P("tp", None),
            P(),
        ),
        out_specs=P(("sp", "tp"), None),
        check_vma=False,
    )
```

profile of v0, /device:TPU:9, one launch (start us, length us, event | category | flops | bytes accessed | tf_op | source)
XLA Modules:
  0.0 56.6 jit_solution(6589171558495436694)
XLA Ops:
  0.0 55.8 %layer.1 = bf16[192,2048]{1,0:T(8,128)(2,1)S(1)} custom-call(bf16[768,512]{1,0:T(8,128)(2,1)} %x_hbm.1, bf16[16,128]{1,0:T(8,128)(2,1)} %bitcast.4, bf16[2048,512]{1,0:T(8,128)(2,1)} %wq_hbm.1, bf16[2048,512]{1,0:T(8,128)(2,1)} %wf_hbm.1, bf16[2048,512]{1,0:T(8,128)(2,1)} %wv_hbm.1, bf16[2048,512]{1,0:T(8,128)(2,1)} %wpre_hbm.1, ...), custom_call_target="tpu_custom_call" | custom-call | tf_op jit(solution)/shard_map/layer/pallas_call | solution.py:561
  55.8 0.9 %copy.19 = bf16[192,2048]{1,0:T(8,128)(2,1)} copy(bf16[192,2048]{1,0:T(8,128)(2,1)S(1)} %layer.1) | data formatting | bytes 1572864
where the time goes:
time: 56.8 us; the launch traced here: 56.6 us
  Pallas kernels  55.8 us (98%)
  local copies, waits for them, and re-layouts  0.88 us (2%)
    pallas_call x1, Pallas kernels, shards(): pl.pallas_call(functools.partial(layer_kernel, heads, chunk, pieces), out...  55.8 us

commit v1 on v0

--- a/solution.py
+++ b/solution.py
@@ -31,6 +31,14 @@
 
 def tn_dot(a, b):
     return lax.dot_general(a, b, (((0,), (0,)), ((), ())), preferred_element_type=F32)
+
+
+def split_terms(logs):
+    high = logs.astype(BF16)
+    rest = logs - high.astype(F32)
+    next_term = rest.astype(BF16)
+    low = (rest - next_term.astype(F32)).astype(BF16)
+    return jnp.concatenate([high, next_term, low], axis=0)
 
 
 def tp_places():
@@ -40,6 +48,19 @@
     cross = 2 * (1 - pair) + core
     far = 2 * (1 - pair) + (1 - core)
     return me, partner, cross, far
+
+
+def owner_place(sp):
+    owners = max(1, sp // 2)
+    return (sp - owners) // 2, sp // owners
+
+
+def outward(low, high):
+    order = []
+    while low <= high:
+        order += [low, high] if low < high else [low]
+        low, high = low + 1, high - 1
+    return order
 
 
 def aligned(start, size):
@@ -85,6 +106,12 @@
     shift,
     st,
     run,
+    raw,
+    carry,
+    pair_land,
+    pair_decs,
+    pair_factor,
+    start_land,
     pack,
     decs,
     land,
@@ -129,8 +156,15 @@
     cs,
     cr,
     ready,
+    ss,
+    sr,
+    qs,
+    qr,
 ):
     peers, tokens, width = xg.shape
+    groups, team = decs.shape[:2]
+    owners, piece = back.shape[0], back.shape[3]
+    first_owner, ratio = owner_place(lax.axis_size("sp"))
     steps = tokens // chunk
     sp = lax.axis_size("sp")
     seq = lax.axis_index("sp")
@@ -201,11 +235,29 @@
     wc_copy.start()
     wr_copy.start()
 
-    def state_hop(src, dst, slot, to, send, recv):
-        return give(src.at[to], dst.at[slot], send.at[to], recv.at[slot], {"sp": to})
-
-    def decay_hop(slot, to):
-        return give(decs, land_decay.at[slot], sd.at[to], rd.at[slot], {"sp": to})
+    own = jnp.clip(seq - first_owner, 0, owners - 1)
+    is_owner = (seq >= first_owner) & (seq < first_owner + owners)
+    start_owner = first_owner + seq // ratio
+
+    def state_hop(g, k, slot, to):
+        return give(pack.at[k, g], land.at[slot, g], s1.at[g, k], r1.at[g, slot], {"sp": to})
+
+    def decay_hop(g, k, slot, to):
+        return give(decs.at[g], land_decay.at[slot, g], sd.at[g, k], rd.at[g, slot], {"sp": to})
+
+    def enter_hop(g, i, slot, to):
+        return give(ent.at[i, g], back.at[slot, g], s2.at[g, to], r2.at[g, slot], {"sp": to})
+
+    def pair_hop():
+        return give(pack, pair_land, qs.at[0], qr.at[0], {"sp": (seq + 1) % sp})
+
+    def pair_decay_hop():
+        return give(decs, pair_decs, qs.at[1], qr.at[1], {"sp": (seq + 1) % sp})
+
+    def start_hop(slot):
+        return give(
+            start_ref, start_land.at[slot], ss.at[0], sr.at[slot], {"sp": start_owner}
+        )
 
     for off in range(1, sp):
         to = (seq + off) % sp
@@ -216,13 +268,6 @@
 
     for copy in small_copies:
         copy.wait()
-    running = [start_ref[h] for h in range(heads)]
-    for h in range(heads):
-        ent[0, h] = running[h].astype(BF16)
-
-    @pl.when(seq > 0)
-    def _():
-        state_hop(ent, back, seq, 0, s2, r2).start()
 
     st[...] = jnp.zeros_like(st)
     run[...] = jnp.zeros_like(run)
@@ -237,12 +282,7 @@
         forget = forget_raw.astype(F32)
         keys = (1.0 - fmin_ref[...]) * jax.nn.sigmoid(-forget)
         logs = jnp.log1p(-keys) + surge[rows, :]
-        high = logs.astype(BF16)
-        rest = logs - high.astype(F32)
-        next_term = rest.astype(BF16)
-        low = (rest - next_term.astype(F32)).astype(BF16)
-        terms = jnp.concatenate([high, next_term, low], axis=0)
-        rel = jnp.dot(middle, terms, preferred_element_type=F32)
+        rel = jnp.dot(middle, split_terms(logs), preferred_element_type=F32)
         mid = logs[0:1, :] - rel[0:1, :]
         tail = rel[BLK - 1 : BLK, :]
         raw = query_raw.astype(F32)
@@ -269,6 +309,36 @@
     def project(rows, j):
         return jnp.dot(nb[rows, :], wbuf[j], preferred_element_type=F32).astype(BF16)
 
+    def blend(rows, now):
+        mix[aligned_by(PAD + now * chunk, PAD, chunk), :] = project(rows, 3).astype(
+            F32
+        ) * project(rows, 4).astype(F32)
+
+    def arrive(now):
+        with jax.named_scope("wait_forward"):
+            hop(now, partner, partner, psend, precv).wait_recv()
+            hop(now, far, partner, fsend, frecv).wait_recv()
+        rows = aligned(now * chunk, chunk)
+        total = jnp.zeros((chunk, 1), F32)
+        for s in range(peers):
+            part_x = xg[s, rows].astype(F32)
+            total = total + jnp.sum(part_x * part_x, axis=-1, keepdims=True)
+        scale = lax.rsqrt(total / (peers * width) + EPS)
+        for s in range(peers):
+            cols = slice(s * width, (s + 1) * width)
+            nb[rows, cols] = (xg[s, rows].astype(F32) * scale * gain[:, cols]).astype(BF16)
+        return rows
+
+    def blocks(now, query_raw, forget_raw, value_raw):
+        for b in range(chunk // BLK):
+            inner = slice(b * BLK, (b + 1) * BLK)
+            block(
+                aligned(now * chunk + b * BLK, BLK),
+                query_raw[inner],
+                forget_raw[inner],
+                value_raw[inner],
+            )
+
     lag = me % 2
 
     @pl.loop(0, steps + lag)
@@ -279,82 +349,140 @@
                 hop(step, cross, cross, csend, crecv).wait_recv()
             hop(step, cross, partner, fsend, frecv).start()
 
-        @pl.when(step >= lag)
+        @pl.when((step >= lag) & (step < steps - 1 + lag))
         def _():
             now = step - lag
-            with jax.named_scope("wait_forward"):
-                hop(now, partner, partner, psend, precv).wait_recv()
-                hop(now, far, partner, fsend, frecv).wait_recv()
-            rows = aligned(now * chunk, chunk)
-            total = jnp.zeros((chunk, 1), F32)
-            for s in range(peers):
-                piece = xg[s, rows].astype(F32)
-                total = total + jnp.sum(piece * piece, axis=-1, keepdims=True)
-            scale = lax.rsqrt(total / (peers * width) + EPS)
-            for s in range(peers):
-                cols = slice(s * width, (s + 1) * width)
-                nb[rows, cols] = (xg[s, rows].astype(F32) * scale * gain[:, cols]).astype(BF16)
+            rows = arrive(now)
 
             @pl.when(now == 0)
             def _():
                 surge_copy.wait()
-                for j in range(3):
+                for j in range(5):
                     weight_copy(j).wait()
 
-            query_raw, forget_raw, value_raw = (project(rows, j) for j in range(3))
-            for b in range(chunk // BLK):
-                inner = slice(b * BLK, (b + 1) * BLK)
-                block(
-                    aligned(now * chunk + b * BLK, BLK),
-                    query_raw[inner],
-                    forget_raw[inner],
-                    value_raw[inner],
+            blocks(now, *(project(rows, j) for j in range(3)))
+            blend(rows, now)
+
+            @pl.when(now == 0)
+            def _():
+                @pl.when(seq < sp - 1)
+                def _():
+                    pl.semaphore_wait(ready, sp - 1 - seq)
+
+                @pl.when(seq != start_owner)
+                def _():
+                    start_hop(seq % ratio).start()
+
+                @pl.when(seq == start_owner)
+                def _():
+                    start_land[seq % ratio] = start_ref[...]
+
+    def enter(i, g):
+        for to in (i,) if i < sp - 2 else (i, i + 1):
+
+            @pl.when(seq != to)
+            def _():
+                enter_hop(g, i, own, to).start()
+
+            @pl.when(seq == to)
+            def _():
+                back[own, g] = ent[i, g]
+
+    @pl.when(is_owner)
+    def _():
+        for r in range(ratio):
+
+            @pl.when(seq != own * ratio + r)
+            def _():
+                start_hop(r).wait_recv()
+
+        for g in range(groups):
+            for t in range(team):
+                running = jnp.concatenate(
+                    [start_land[r, g * team + t] for r in range(ratio)], axis=0
                 )
-
-    piece = DK // sp
+                carry[g, t] = running
+                ent[0, g, t] = running.astype(BF16)
+        for g in range(groups):
+            enter(0, g)
+
+    final = steps - 1
+    rows = arrive(final)
     packing = jax.named_scope("pack")
     packing.__enter__()
-    whole = jnp.exp(run[...])
-    for h in range(heads):
-        ch = slice(h * DK, (h + 1) * DK)
-        decs[h : h + 1, :] = whole[:, ch]
-        state = st[h].T
-        for p in range(sp):
-            pack[p, h] = state[p * piece : (p + 1) * piece].astype(BF16)
-
-    @pl.when(seq < sp - 1)
-    def _():
-        pl.semaphore_wait(ready, sp - 1 - seq)
-        for off in range(1, sp):
-            to = (seq + off) % sp
-            decay_hop(seq, to).start()
-            state_hop(pack, land, seq, to, s1, r1).start()
-
-    land[seq] = pack[seq]
-    land_decay[seq] = decs[...]
+    span = team * DK
+    row = lax.broadcasted_iota(jnp.int32, (chunk, chunk), 0)
+    col = lax.broadcasted_iota(jnp.int32, (chunk, chunk), 1)
+    later = (col > row).astype(F32).astype(BF16)
+    later = jnp.concatenate([later] * 3, axis=1)
+    raw[0], raw[1] = project(rows, 1), project(rows, 2)
+    for g in range(groups):
+        cols = slice(g * span, (g + 1) * span)
+        forget_raw, value_raw = raw[0, :, cols], raw[1, :, cols]
+        keys = (1.0 - fmin_ref[:, cols]) * jax.nn.sigmoid(-forget_raw.astype(F32))
+        logs = jnp.log1p(-keys) + surge[rows, cols]
+        after = jnp.dot(later, split_terms(logs), preferred_element_type=F32)
+        total = after[0:1, :] + logs[0:1, :]
+        k_out = (keys * jnp.exp(after)).astype(BF16)
+        whole = jnp.exp(total)
+        gone = jnp.exp(run[:, cols] + total)
+        for t in range(team):
+            ch = slice(t * DK, (t + 1) * DK)
+            decs[g, t : t + 1, :] = gone[:, ch]
+            state = st[g * team + t] * whole[:, ch] + tn_dot(value_raw[:, ch], k_out[:, ch])
+            state = state.T
+            for k in range(owners):
+                pack[k, g, t] = state[k * piece : (k + 1) * piece].astype(BF16)
+
+        @pl.when(seq < sp - 2)
+        def _():
+            for k in range(owners):
+
+                @pl.when(seq != first_owner + k)
+                def _():
+                    decay_hop(g, k, seq, first_owner + k).start()
+                    state_hop(g, k, seq, first_owner + k).start()
+
+    @pl.when(seq == sp - 2)
+    def _():
+        pair_decay_hop().start()
+        pair_hop().start()
+
+    @pl.when(is_owner & (seq < sp - 2))
+    def _():
+        land[seq] = pack[own]
+        land_decay[seq] = decs[...]
+
     packing.__exit__(None, None, None)
+
+    def combine(g, low, high):
+        with jax.named_scope("wait_states"):
+            for i in range(low, high):
+
+                @pl.when(seq != i)
+                def _():
+                    decay_hop(g, 0, i, seq).wait_recv()
+                    state_hop(g, 0, i, seq).wait_recv()
+
+        lane = lax.broadcasted_iota(jnp.int32, (piece, DK), 1)
+        pick = lane == own * piece + lax.broadcasted_iota(jnp.int32, (piece, DK), 0)
+        for t in range(team):
+            running = carry[g, t]
+            for i in range(low, high):
+                line = jnp.broadcast_to(land_decay[i, g, t : t + 1, :], (piece, DK))
+                decay = jnp.sum(jnp.where(pick, line, 0.0), axis=-1, keepdims=True)
+                running = decay * running + land[i, g, t].astype(F32)
+                ent[i + 1, g, t] = running.astype(BF16)
+            carry[g, t] = running
+        for i in outward(low + 1, high):
+            enter(i, g)
+
     gates = jax.named_scope("gates_a")
     gates.__enter__()
-    for j in range(3, 7):
+    for j in range(5, 7):
         weight_copy(j).wait()
-
-    def halo_hop():
-        return give(
-            mix.at[pl.ds(tokens, PAD)], halo, hs.at[0], hr.at[0], {"sp": (seq + 1) % sp}
-        )
-
-    wide = 2 * chunk if tokens % (2 * chunk) == 0 else chunk
-
-    @pl.loop(0, tokens // wide)
-    def _(i):
-        rows = aligned(i * wide, wide)
-        mix[pl.ds(pl.multiple_of(PAD + i * wide, PAD), wide), :] = project(rows, 3).astype(
-            F32
-        ) * project(rows, 4).astype(F32)
-
-    @pl.when(seq < sp - 1)
-    def _():
-        halo_hop().start()
+    blocks(final, project(rows, 0), raw[0], raw[1])
+    blend(rows, final)
 
     def prepare(which):
         rows = aligned(which * quarter, quarter)
@@ -372,35 +500,27 @@
         conv = (post[rows, :].astype(F32) * total).astype(BF16)
         acc[rows, :] = jnp.dot(conv, wc[...], preferred_element_type=F32)
 
+    def halo_hop():
+        return give(
+            mix.at[pl.ds(tokens, PAD)], halo, hs.at[0], hr.at[0], {"sp": (seq + 1) % sp}
+        )
+
+    @pl.when(seq < sp - 1)
+    def _():
+        halo_hop().start()
+
     prepare(far)
     gates.__exit__(None, None, None)
-    with jax.named_scope("wait_states"):
-        for off in range(1, sp):
-            src = (seq + sp - off) % sp
-
-            @pl.when(src < sp - 1)
-            def _():
-                decay_hop(src, (seq + off) % sp).wait_recv()
-                state_hop(pack, land, src, (seq + off) % sp, s1, r1).wait_recv()
-
-    gates = jax.named_scope("gates_b")
+
+    @pl.when(is_owner)
+    def _():
+        split = sp // 4
+        for low, high in ((0, split), (split, sp - 2)):
+            for g in range(groups):
+                combine(g, low, high)
+
+    gates = jax.named_scope("gates_c")
     gates.__enter__()
-    lane = lax.broadcasted_iota(jnp.int32, (piece, DK), 1)
-    pick = lane == seq * piece + lax.broadcasted_iota(jnp.int32, (piece, DK), 0)
-    for i in range(sp - 1):
-        for h in range(heads):
-            line = jnp.broadcast_to(land_decay[i, h : h + 1, :], (piece, DK))
-            decay = jnp.sum(jnp.where(pick, line, 0.0), axis=-1, keepdims=True)
-            running[h] = decay * running[h] + land[i, h].astype(F32)
-            ent[i + 1, h] = running[h].astype(BF16)
-    back[seq] = ent[seq]
-    for off in range(1, sp):
-        to = (seq + off) % sp
-
-        @pl.when(to > 0)
-        def _():
-            state_hop(ent, back, seq, to, s2, r2).start()
-
     prepare(cross)
     mix[0:PAD, :] = jnp.zeros((PAD, width), F32)
 
@@ -414,14 +534,38 @@
     convolve(far)
     convolve(cross)
     gates.__exit__(None, None, None)
+    def whole_state(pieces_ref, h):
+        return jnp.concatenate(
+            [pieces_ref[k, h // team, h % team].astype(F32) for k in range(owners)], axis=0
+        )
+
+    @pl.when(seq == sp - 1)
+    def _():
+        pair_decay_hop().wait_recv()
+        pair_hop().wait_recv()
+        for h in range(heads):
+            line = pair_decs[h // team, h % team : h % team + 1, :]
+            pair_factor[h] = jnp.broadcast_to(line, (DV, DK)).T
+
     with jax.named_scope("wait_entering"):
-        for off in range(1, sp):
-            src = (seq + sp - off) % sp
-            state_hop(ent, back, src, (seq + off) % sp, s2, r2).wait_recv()
-    for h in range(heads):
-        land_state[h] = jnp.concatenate(
-            [back[i, h].astype(F32) for i in range(sp)], axis=0
-        ).astype(BF16)
+        for g in range(groups):
+            for k in range(owners):
+
+                @pl.when(seq != first_owner + k)
+                def _():
+                    enter_hop(g, 0, k, 0).wait_recv()
+
+    @pl.when(seq < sp - 1)
+    def _():
+        for h in range(heads):
+            land_state[h] = whole_state(back, h).astype(BF16)
+
+    @pl.when(seq == sp - 1)
+    def _():
+        for h in range(heads):
+            land_state[h] = (
+                pair_factor[h] * whole_state(back, h) + whole_state(pair_land, h)
+            ).astype(BF16)
 
     def mixed(which, s):
         rows = aligned(which * quarter + s * size, size)
@@ -505,15 +649,33 @@
         hop(step, me, cross, csend, crecv).wait_send()
         hop(step, me, partner, psend, precv).wait_send()
         hop(step, cross, partner, fsend, frecv).wait_send()
-    for off in range(1, sp):
-        to = (seq + off) % sp
-
-        @pl.when(seq < sp - 1)
-        def _():
-            decay_hop(seq, to).wait_send()
-            state_hop(pack, land, seq, to, s1, r1).wait_send()
-
-        state_hop(ent, back, seq, to, s2, r2).wait_send()
+    @pl.when(seq < sp - 2)
+    def _():
+        for g in range(groups):
+            for k in range(owners):
+
+                @pl.when(seq != first_owner + k)
+                def _():
+                    decay_hop(g, k, seq, first_owner + k).wait_send()
+                    state_hop(g, k, seq, first_owner + k).wait_send()
+
+    @pl.when(seq == sp - 2)
+    def _():
+        pair_decay_hop().wait_send()
+        pair_hop().wait_send()
+
+    @pl.when(is_owner)
+    def _():
+        for g in range(groups):
+            for i in range(sp):
+
+                @pl.when(seq != i)
+                def _():
+                    enter_hop(g, 0, own, i).wait_send()
+
+    @pl.when(seq != start_owner)
+    def _():
+        start_hop(seq % ratio).wait_send()
 
     @pl.when(seq < sp - 1)
     def _():
@@ -554,7 +716,11 @@
     quarter = tokens // tp
     pieces = 4 if quarter % 64 == 0 else 2
     size = quarter // pieces
-    shares = (sp, heads, DK // sp, DV)
+    _, ratio = owner_place(sp)
+    owners = sp // ratio
+    groups = 2 if heads % 2 == 0 else 1
+    team = heads // groups
+    share = (groups, team, DK // owners, DV)
     vmem = pl.BlockSpec(memory_space=pltpu.VMEM)
     hbm = pl.BlockSpec(memory_space=pltpu.HBM)
     dma = pltpu.SemaphoreType.DMA
@@ -572,12 +738,18 @@
             pltpu.VMEM((tokens, cols), BF16),
             pltpu.VMEM((heads, DV, DK), F32),
             pltpu.VMEM((1, cols), F32),
-            pltpu.VMEM(shares, BF16),
-            pltpu.VMEM((heads, DK), F32),
-            pltpu.VMEM(shares, BF16),
-            pltpu.VMEM((sp, heads, DK), F32),
-            pltpu.VMEM(shares, BF16),
-            pltpu.VMEM(shares, BF16),
+            pltpu.VMEM((2, chunk, cols), BF16),
+            pltpu.VMEM(share, F32),
+            pltpu.VMEM((owners,) + share, BF16),
+            pltpu.VMEM((groups, team, DK), F32),
+            pltpu.VMEM((heads, DK, DV), F32),
+            pltpu.VMEM((ratio,) + starting_state.shape, F32),
+            pltpu.VMEM((owners,) + share, BF16),
+            pltpu.VMEM((groups, team, DK), F32),
+            pltpu.VMEM((sp,) + share, BF16),
+            pltpu.VMEM((sp, groups, team, DK), F32),
+            pltpu.VMEM((sp - 1,) + share, BF16),
+            pltpu.VMEM((owners,) + share, BF16),
             pltpu.VMEM((tokens, cols), BF16),
             pltpu.VMEM((tokens, cols), BF16),
             pltpu.VMEM((tokens + PAD, cols), F32),
@@ -599,11 +771,13 @@
             dma((17,)),
         ]
         + [dma((steps,))] * 6
-        + [dma((sp,))] * 6
+        + [dma((groups, owners)), dma((groups, sp))] * 2
+        + [dma((groups, sp)), dma((groups, owners))]
         + [dma((1,))] * 2
         + [dma((2 * pieces,))] * 2
         + [dma((pieces,))] * 2
-        + [pltpu.SemaphoreType.REGULAR],
+        + [pltpu.SemaphoreType.REGULAR]
+        + [dma((1,)), dma((ratio,)), dma((2,)), dma((2,))],
         compiler_params=pltpu.CompilerParams(collective_id=0, has_side_effects=True, vmem_limit_bytes=56 * 1024 * 1024),
         name="layer",
     )(

time: 56.8 us -> 55.3 us (0.974)
  Pallas kernels: 55.8 us -> 54.2 us
    pallas_call x1, Pallas kernels: 55.8 us -> 54.2 us  [shards(): pl.pallas_call(functools.partial(layer_kernel, heads, chunk, pieces), out...]
where the time goes in v1:
time: 55.3 us; the launch traced here: 55 us
  Pallas kernels  54.2 us (98%)
  local copies, waits for them, and re-layouts  0.88 us (2%)
    pallas_call x1, Pallas kernels, shards(): pl.pallas_call(functools.partial(layer_kernel, heads, chunk, pieces), out...  54.2 us

profile of v1, /device:TPU:9, one launch (start us, length us, event | category | flops | bytes accessed | tf_op | source)
XLA Modules:
  0.0 55.0 jit_solution(4902497081035438619)
XLA Ops:
  0.0 54.2 %layer.1 = bf16[192,2048]{1,0:T(8,128)(2,1)S(1)} custom-call(bf16[768,512]{1,0:T(8,128)(2,1)} %x_hbm.1, bf16[16,128]{1,0:T(8,128)(2,1)} %bitcast.4, bf16[2048,512]{1,0:T(8,128)(2,1)} %wq_hbm.1, bf16[2048,512]{1,0:T(8,128)(2,1)} %wf_hbm.1, bf16[2048,512]{1,0:T(8,128)(2,1)} %wv_hbm.1, bf16[2048,512]{1,0:T(8,128)(2,1)} %wpre_hbm.1, ...), custom_call_target="tpu_custom_call" | custom-call | tf_op jit(solution)/shard_map/layer/pallas_call | solution.py:727
  54.2 0.9 %copy.19 = bf16[192,2048]{1,0:T(8,128)(2,1)} copy(bf16[192,2048]{1,0:T(8,128)(2,1)S(1)} %layer.1) | data formatting | bytes 1572864

commit v2 on v1

--- a/solution.py
+++ b/solution.py
@@ -224,12 +224,17 @@
 
     def hop(step, slot, to, send, recv):
         rows = aligned(step * chunk, chunk)
-        return give(xg.at[slot, rows], xg.at[slot, rows], send.at[step], recv.at[step], {"tp": to})
+        return give(xg.at[slot, rows], xg.at[slot, rows], send.at[0], recv.at[step], {"tp": to})
+
+    def sent(slot, to, send, recv):
+        give(xg.at[slot], xg.at[slot], send.at[0], recv.at[0], {"tp": to}).wait_send()
+
+    def partner_copy(slot):
+        return give(xg.at[slot], xg.at[slot], psend.at[0], precv.at[0], {"tp": partner})
 
     for step in range(steps):
         hop(step, me, cross, csend, crecv).start()
-    for step in range(steps):
-        hop(step, me, partner, psend, precv).start()
+    partner_copy(me).start()
     for j in range(3, 7):
         weight_copy(j).start()
     wc_copy.start()
@@ -239,14 +244,21 @@
     is_owner = (seq >= first_owner) & (seq < first_owner + owners)
     start_owner = first_owner + seq // ratio
 
+    split = sp // 4
+
+    def stage_of(slot):
+        return jnp.where(slot < split, 0, 1)
+
     def state_hop(g, k, slot, to):
-        return give(pack.at[k, g], land.at[slot, g], s1.at[g, k], r1.at[g, slot], {"sp": to})
-
-    def decay_hop(g, k, slot, to):
-        return give(decs.at[g], land_decay.at[slot, g], sd.at[g, k], rd.at[g, slot], {"sp": to})
+        return give(
+            pack.at[k, g], land.at[slot, g], s1.at[0], r1.at[g, stage_of(slot)], {"sp": to}
+        )
+
+    def decay_hop(slot, to):
+        return give(decs, land_decay.at[slot], sd.at[0], rd.at[stage_of(slot)], {"sp": to})
 
     def enter_hop(g, i, slot, to):
-        return give(ent.at[i, g], back.at[slot, g], s2.at[g, to], r2.at[g, slot], {"sp": to})
+        return give(ent.at[i, g], back.at[slot, g], s2.at[0], r2.at[0], {"sp": to})
 
     def pair_hop():
         return give(pack, pair_land, qs.at[0], qr.at[0], {"sp": (seq + 1) % sp})
@@ -316,13 +328,13 @@
 
     def arrive(now):
         with jax.named_scope("wait_forward"):
-            hop(now, partner, partner, psend, precv).wait_recv()
             hop(now, far, partner, fsend, frecv).wait_recv()
         rows = aligned(now * chunk, chunk)
-        total = jnp.zeros((chunk, 1), F32)
+        squares = jnp.zeros((chunk, width), F32)
         for s in range(peers):
             part_x = xg[s, rows].astype(F32)
-            total = total + jnp.sum(part_x * part_x, axis=-1, keepdims=True)
+            squares = squares + part_x * part_x
+        total = jnp.sum(squares, axis=-1, keepdims=True)
         scale = lax.rsqrt(total / (peers * width) + EPS)
         for s in range(peers):
             cols = slice(s * width, (s + 1) * width)
@@ -352,16 +364,19 @@
         @pl.when((step >= lag) & (step < steps - 1 + lag))
         def _():
             now = step - lag
-            rows = arrive(now)
-
             @pl.when(now == 0)
             def _():
+                partner_copy(partner).wait_recv()
                 surge_copy.wait()
                 for j in range(5):
                     weight_copy(j).wait()
 
+            rows = arrive(now)
             blocks(now, *(project(rows, j) for j in range(3)))
-            blend(rows, now)
+
+            @pl.when(now < steps // 2)
+            def _():
+                blend(rows, now)
 
             @pl.when(now == 0)
             def _():
@@ -416,19 +431,29 @@
     later = (col > row).astype(F32).astype(BF16)
     later = jnp.concatenate([later] * 3, axis=1)
     raw[0], raw[1] = project(rows, 1), project(rows, 2)
+    keys = (1.0 - fmin_ref[...]) * jax.nn.sigmoid(-raw[0].astype(F32))
+    logs = jnp.log1p(-keys) + surge[rows, :]
+    after = jnp.dot(later, split_terms(logs), preferred_element_type=F32)
+    total = after[0:1, :] + logs[0:1, :]
+    k_all = (keys * jnp.exp(after)).astype(BF16)
+    whole_all = jnp.exp(total)
+    gone = jnp.exp(run[...] + total)
+    for h in range(heads):
+        decs[h // team, h % team : h % team + 1, :] = gone[:, h * DK : (h + 1) * DK]
+
+    @pl.when(seq < sp - 2)
+    def _():
+        for k in range(owners):
+
+            @pl.when(seq != first_owner + k)
+            def _():
+                decay_hop(seq, first_owner + k).start()
+
     for g in range(groups):
         cols = slice(g * span, (g + 1) * span)
-        forget_raw, value_raw = raw[0, :, cols], raw[1, :, cols]
-        keys = (1.0 - fmin_ref[:, cols]) * jax.nn.sigmoid(-forget_raw.astype(F32))
-        logs = jnp.log1p(-keys) + surge[rows, cols]
-        after = jnp.dot(later, split_terms(logs), preferred_element_type=F32)
-        total = after[0:1, :] + logs[0:1, :]
-        k_out = (keys * jnp.exp(after)).astype(BF16)
-        whole = jnp.exp(total)
-        gone = jnp.exp(run[:, cols] + total)
+        value_raw, k_out, whole = raw[1, :, cols], k_all[:, cols], whole_all[:, cols]
         for t in range(team):
             ch = slice(t * DK, (t + 1) * DK)
-            decs[g, t : t + 1, :] = gone[:, ch]
             state = st[g * team + t] * whole[:, ch] + tn_dot(value_raw[:, ch], k_out[:, ch])
             state = state.T
             for k in range(owners):
@@ -440,7 +465,6 @@
 
                 @pl.when(seq != first_owner + k)
                 def _():
-                    decay_hop(g, k, seq, first_owner + k).start()
                     state_hop(g, k, seq, first_owner + k).start()
 
     @pl.when(seq == sp - 2)
@@ -457,12 +481,24 @@
 
     def combine(g, low, high):
         with jax.named_scope("wait_states"):
-            for i in range(low, high):
-
-                @pl.when(seq != i)
-                def _():
-                    decay_hop(g, 0, i, seq).wait_recv()
-                    state_hop(g, 0, i, seq).wait_recv()
+            stage = 0 if low < split else 1
+            inside = (seq >= low) & (seq < high)
+
+            def waits(count):
+                if g == 0 and count > 0:
+                    lines = land_decay.at[pl.ds(0, count)]
+                    give(lines, lines, sd.at[0], rd.at[stage], {"sp": seq}).wait_recv()
+                if count > 0:
+                    parts = land.at[pl.ds(0, count), g]
+                    give(parts, parts, s1.at[0], r1.at[g, stage], {"sp": seq}).wait_recv()
+
+            @pl.when(inside)
+            def _():
+                waits(high - low - 1)
+
+            @pl.when(jnp.logical_not(inside))
+            def _():
+                waits(high - low)
 
         lane = lax.broadcasted_iota(jnp.int32, (piece, DK), 1)
         pick = lane == own * piece + lax.broadcasted_iota(jnp.int32, (piece, DK), 0)
@@ -514,7 +550,6 @@
 
     @pl.when(is_owner)
     def _():
-        split = sp // 4
         for low, high in ((0, split), (split, sp - 2)):
             for g in range(groups):
                 combine(g, low, high)
@@ -522,6 +557,10 @@
     gates = jax.named_scope("gates_c")
     gates.__enter__()
     prepare(cross)
+    @pl.loop(steps // 2, final)
+    def _(now):
+        blend(aligned(now * chunk, chunk), now)
+
     mix[0:PAD, :] = jnp.zeros((PAD, width), F32)
 
     @pl.when(seq > 0)
@@ -548,12 +587,18 @@
             pair_factor[h] = jnp.broadcast_to(line, (DV, DK)).T
 
     with jax.named_scope("wait_entering"):
-        for g in range(groups):
-            for k in range(owners):
-
-                @pl.when(seq != first_owner + k)
-                def _():
-                    enter_hop(g, 0, k, 0).wait_recv()
+        def entered(count):
+            if count > 0:
+                parts = back.at[pl.ds(0, count)]
+                give(parts, parts, s2.at[0], r2.at[0], {"sp": seq}).wait_recv()
+
+        @pl.when(is_owner)
+        def _():
+            entered(owners - 1)
+
+        @pl.when(jnp.logical_not(is_owner))
+        def _():
+            entered(owners)
 
     @pl.when(seq < sp - 1)
     def _():
@@ -589,10 +634,10 @@
         acc[rows, :] = mixed(which, s)
 
     def partner_hop(i):
-        return give(pbuf.at[i], prcv.at[i], ps.at[i], pr.at[i], {"tp": partner})
+        return give(pbuf.at[i], prcv.at[i], ps.at[0], pr.at[i], {"tp": partner})
 
     def cross_hop(i):
-        return give(cbuf.at[i], crcv.at[i], cs.at[i], cr.at[i], {"tp": cross})
+        return give(cbuf.at[i], crcv.at[i], cs.at[0], cr.at[i], {"tp": cross})
 
     def share(which, s, slot):
         pbuf[slot] = mixed(which, s).astype(BF16)
@@ -632,6 +677,42 @@
         put(me, s)
 
     sums.__exit__(None, None, None)
+    sent(me, cross, csend, crecv)
+    sent(me, partner, psend, precv)
+    sent(cross, partner, fsend, frecv)
+
+    def states_sent(count):
+        if count > 0:
+            parts, lines = pack.at[pl.ds(0, count)], land_decay.at[pl.ds(0, count)]
+            give(lines, lines, sd.at[0], rd.at[0], {"sp": seq}).wait_send()
+            give(parts, parts, s1.at[0], r1.at[0, 0], {"sp": seq}).wait_send()
+
+    @pl.when((seq < sp - 2) & is_owner)
+    def _():
+        states_sent(owners - 1)
+
+    @pl.when((seq < sp - 2) & jnp.logical_not(is_owner))
+    def _():
+        states_sent(owners)
+
+    @pl.when(seq == sp - 2)
+    def _():
+        pair_decay_hop().wait_send()
+        pair_hop().wait_send()
+
+    @pl.when(is_owner)
+    def _():
+        give(ent, ent, s2.at[0], r2.at[0], {"sp": seq}).wait_send()
+
+    @pl.when(seq != start_owner)
+    def _():
+        start_hop(seq % ratio).wait_send()
+
+    @pl.when(seq < sp - 1)
+    def _():
+        halo_hop().wait_send()
+
+    give(pbuf, prcv, ps.at[0], pr.at[0], {"tp": partner}).wait_send()
     last = jax.named_scope("last")
     last.__enter__()
     ogain = row_of(ogain_ref)
@@ -645,46 +726,8 @@
         out_ref[aligned(s * size, size), :] = (total * rms_scale(total) * ogain).astype(BF16)
 
     last.__exit__(None, None, None)
-    for step in range(steps):
-        hop(step, me, cross, csend, crecv).wait_send()
-        hop(step, me, partner, psend, precv).wait_send()
-        hop(step, cross, partner, fsend, frecv).wait_send()
-    @pl.when(seq < sp - 2)
-    def _():
-        for g in range(groups):
-            for k in range(owners):
-
-                @pl.when(seq != first_owner + k)
-                def _():
-                    decay_hop(g, k, seq, first_owner + k).wait_send()
-                    state_hop(g, k, seq, first_owner + k).wait_send()
-
-    @pl.when(seq == sp - 2)
-    def _():
-        pair_decay_hop().wait_send()
-        pair_hop().wait_send()
-
-    @pl.when(is_owner)
-    def _():
-        for g in range(groups):
-            for i in range(sp):
-
-                @pl.when(seq != i)
-                def _():
-                    enter_hop(g, 0, own, i).wait_send()
-
-    @pl.when(seq != start_owner)
-    def _():
-        start_hop(seq % ratio).wait_send()
-
-    @pl.when(seq < sp - 1)
-    def _():
-        halo_hop().wait_send()
-
-    for i in range(2 * pieces):
-        partner_hop(i).wait_send()
-    for i in range(pieces):
-        cross_hop(i).wait_send()
+    with jax.named_scope("sends"):
+        give(cbuf, crcv, cs.at[0], cr.at[0], {"tp": cross}).wait_send()
 
 
 def shards(
@@ -770,12 +813,10 @@
             pltpu.VMEM((wide // LANES, LANES), BF16),
             dma((17,)),
         ]
-        + [dma((steps,))] * 6
-        + [dma((groups, owners)), dma((groups, sp))] * 2
-        + [dma((groups, sp)), dma((groups, owners))]
+        + [dma((1,)), dma((steps,)), dma((1,)), dma((1,)), dma((1,)), dma((steps,))]
+        + [dma((1,)), dma((groups, 2)), dma((1,)), dma((2,)), dma((1,)), dma((1,))]
         + [dma((1,))] * 2
-        + [dma((2 * pieces,))] * 2
-        + [dma((pieces,))] * 2
+        + [dma((1,)), dma((2 * pieces,)), dma((1,)), dma((pieces,))]
         + [pltpu.SemaphoreType.REGULAR]
         + [dma((1,)), dma((ratio,)), dma((2,)), dma((2,))],
         compiler_params=pltpu.CompilerParams(collective_id=0, has_side_effects=True, vmem_limit_bytes=56 * 1024 * 1024),

time: 55.3 us -> 53.8 us (0.973)
  Pallas kernels: 54.2 us -> 52.5 us
    pallas_call x1, Pallas kernels: 54.2 us -> 52.5 us  [shards(): pl.pallas_call(functools.partial(layer_kernel, heads, chunk, pieces), out...]
where the time goes in v2:
time: 53.8 us; the launch traced here: 53.4 us
  Pallas kernels  52.5 us (98%)
  local copies, waits for them, and re-layouts  0.88 us (2%)
    pallas_call x1, Pallas kernels, shards(): pl.pallas_call(functools.partial(layer_kernel, heads, chunk, pieces), out...  52.5 us

profile of v2, /device:TPU:9, one launch (start us, length us, event | category | flops | bytes accessed | tf_op | source)
XLA Modules:
  0.0 53.4 jit_solution(16483550417821252429)
XLA Ops:
  0.0 52.5 %layer.1 = bf16[192,2048]{1,0:T(8,128)(2,1)S(1)} custom-call(bf16[768,512]{1,0:T(8,128)(2,1)} %x_hbm.1, bf16[16,128]{1,0:T(8,128)(2,1)} %bitcast.4, bf16[2048,512]{1,0:T(8,128)(2,1)} %wq_hbm.1, bf16[2048,512]{1,0:T(8,128)(2,1)} %wf_hbm.1, bf16[2048,512]{1,0:T(8,128)(2,1)} %wv_hbm.1, bf16[2048,512]{1,0:T(8,128)(2,1)} %wpre_hbm.1, ...), custom_call_target="tpu_custom_call" | custom-call | tf_op jit(solution)/shard_map/layer/pallas_call | solution.py:770
  52.5 0.9 %copy.19 = bf16[192,2048]{1,0:T(8,128)(2,1)} copy(bf16[192,2048]{1,0:T(8,128)(2,1)S(1)} %layer.1) | data formatting | bytes 1572864
